TPU v7x, 32 devices: a whole 2x2x4 slice. The times are simulated.
32 devices in a mesh: ep: 16 (over z, x, core), tp: 2 (over y).
Axes of the slice: x: 2, y: 2, z: 4, core: 2. Of those that a mesh axis runs over, the one named last changes fastest.
Arguments:
- tokens: bfloat16 [256, 1024], P('ep'), may hold values from -6 to 6
- old_state: float32 [256, 4, 128, 128], P('ep', 'tp'), may hold values from -6 to 6
- query_weight: bfloat16 [1024, 512], P(None, 'tp'), may hold values from -0.1875 to 0.1875
- forget_weight: bfloat16 [1024, 512], P(None, 'tp'), may hold values from -0.1875 to 0.1875
- input_weight: bfloat16 [1024, 512], P(None, 'tp'), may hold values from -0.1875 to 0.1875
- lower_bound: float32 [512], P('tp'), may hold values from 0 to 0.9
- head_gain: float32 [4, 128], P('tp'), may hold values from 0.1 to 1.9
- out_weight: bfloat16 [512, 1024], P('tp'), may hold values from -0.25 to 0.25
- mix_gain: float32 [1024], replicated, may hold values from 0.1 to 1.9
- ffn_gain: float32 [1024], replicated, may hold values from 0.1 to 1.9
- group_weight: bfloat16 [1024, 4], replicated, may hold values from -0.1875 to 0.1875
- expert_weight: bfloat16 [1024, 16], replicated, may hold values from -0.1875 to 0.1875
- routes: int32 [256, 6], P('ep'), may hold values from 0 to 15, all different within a row; in each aligned block of 16 rows (0 to 15, 16 to 31, ...) at most 12 rows name the same one
- gate_weight: bfloat16 [16, 1024, 1024], P('ep', None, 'tp'), may hold values from -0.1875 to 0.1875
- up_weight: bfloat16 [16, 1024, 1024], P('ep', None, 'tp'), may hold values from -0.1875 to 0.1875
- down_weight: bfloat16 [16, 1024, 1024], P('ep', None, 'tp'), may hold values from -0.1875 to 0.1875
Outputs:
- layer_out: bfloat16 [256, 1024], P('ep', 'tp')
- new_state: float32 [256, 4, 128, 128], P('ep', 'tp')
Inputs may be any that keep to these rules, and one draw needn't show every extreme that they name: `routes`: each row names 6 different experts. In each aligned block of 16 rows (the rows of one device) no expert is named more than 12 times, a bound that some block reaches.
All inputs are finite; a program needn't handle non-finite values.
Results may differ from a plain program's by a relative error of at most 0.011.
Values may be sent and summed in bfloat16 or wider, within the bound.
A program may use at most 64 MiB of HBM per device.

v0:
```python
import jax
import jax.numpy as jnp
from jax import lax
from jax.sharding import PartitionSpec as P

epsilon = 1e-06


def scaled_rms(values, gain):
    return values * lax.rsqrt(jnp.mean(values * values, axis=-1, keepdims=True) + epsilon) * gain


def local(
    tokens,
    old_state,
    query_weight,
    forget_weight,
    input_weight,
    lower_bound,
    head_gain,
    out_weight,
    mix_gain,
    ffn_gain,
    group_weight,
    expert_weight,
    routes,
    gate_weight,
    up_weight,
    down_weight,
):
    seq_count, model_width = tokens.shape
    heads_local, head_size = (old_state.shape[1], old_state.shape[2])
    tp_size = lax.axis_size("tp")
    tp_rank = lax.axis_index("tp")
    part_width = model_width // tp_size
    resident = tokens.astype(jnp.float32)
    normed = scaled_rms(resident, mix_gain).astype(jnp.bfloat16)
    query_pre = jnp.dot(normed, query_weight, preferred_element_type=jnp.float32)
    forget_pre = jnp.dot(normed, forget_weight, preferred_element_type=jnp.float32)
    input_pre = jnp.dot(normed, input_weight, preferred_element_type=jnp.float32)
    query = jax.nn.silu(query_pre).reshape(seq_count, heads_local, head_size)
    forget = (lower_bound + (1.0 - lower_bound) * jax.nn.sigmoid(forget_pre)).reshape(
        seq_count, heads_local, head_size
    )
    value = input_pre.reshape(seq_count, heads_local, head_size)
    new_state = forget[..., None] * old_state + (1.0 - forget)[..., None] * value[:, :, None, :]
    readout = jnp.sum(new_state * query[..., None], axis=2)
    head_out = (
        scaled_rms(readout, head_gain)
        .astype(jnp.bfloat16)
        .reshape(seq_count, heads_local * head_size)
    )
    head_part = jnp.dot(head_out, out_weight, preferred_element_type=jnp.float32)
    mixed = lax.psum(head_part.astype(jnp.bfloat16), "tp")
    residual = (resident + mixed.astype(jnp.float32)).astype(jnp.bfloat16)
    ffn_in = scaled_rms(residual.astype(jnp.float32), ffn_gain).astype(jnp.bfloat16)
    experts = expert_weight.shape[1]
    groups = group_weight.shape[1]
    top_count = routes.shape[1]
    group_raw = jnp.exp(jnp.dot(ffn_in, group_weight, preferred_element_type=jnp.float32))
    group_prob = group_raw / jnp.sum(group_raw, axis=-1, keepdims=True)
    expert_raw = jnp.exp(
        jnp.dot(ffn_in, expert_weight, preferred_element_type=jnp.float32)
    ).reshape(seq_count, groups, experts // groups)
    expert_prob = (
        expert_raw / jnp.sum(expert_raw, axis=-1, keepdims=True) * group_prob[:, :, None]
    ).reshape(seq_count, experts)
    expert_ids = jnp.arange(experts, dtype=jnp.int32)
    chosen = routes[:, :, None] == expert_ids[None, None, :]
    weight = jnp.sum(jnp.where(chosen, expert_prob[:, None, :], 0.0), axis=-1)
    gate = weight / jnp.sum(weight, axis=-1, keepdims=True)
    capacity = min(seq_count, max(2, 2 * seq_count * top_count // experts))
    flat = routes.reshape(-1)
    hits = (flat[:, None] == expert_ids[None, :]).astype(jnp.int32)
    before = jnp.cumsum(hits, axis=0) - hits
    slots = jnp.sum(hits * before, axis=1)
    target = flat * capacity + slots
    slot_ids = jnp.arange(experts * capacity, dtype=jnp.int32)
    spread = jnp.sum(
        (slot_ids[:, None, None] == target.reshape(seq_count, top_count)[None, :, :]).astype(
            jnp.int32
        ),
        axis=2,
    ).astype(jnp.bfloat16)
    choose = (target[:, None] == slot_ids[None, :]).astype(jnp.bfloat16)
    outgoing = (
        jnp.dot(spread, ffn_in, preferred_element_type=jnp.float32)
        .astype(jnp.bfloat16)
        .reshape(experts, capacity, model_width)
    )
    arrived = lax.all_to_all(outgoing, "ep", split_axis=0, concat_axis=1, tiled=True)
    gate_hidden = jnp.einsum(
        "erd,edf->erf", arrived, gate_weight, preferred_element_type=jnp.float32
    )
    up_hidden = jnp.einsum("erd,edf->erf", arrived, up_weight, preferred_element_type=jnp.float32)
    hidden = (jax.nn.silu(gate_hidden) * up_hidden).astype(jnp.bfloat16)
    produced = jnp.einsum(
        "erf,efd->erd",
        lax.all_gather(hidden, "tp", axis=2, tiled=True),
        down_weight,
        preferred_element_type=jnp.float32,
    ).astype(jnp.bfloat16)
    returned = lax.all_to_all(produced, "ep", split_axis=1, concat_axis=0, tiled=True)
    picked = jnp.dot(
        choose, returned.reshape(experts * capacity, part_width), preferred_element_type=jnp.float32
    ).reshape(seq_count, top_count, part_width)
    mixture = jnp.sum(gate[:, :, None] * picked, axis=1)
    own_resid = lax.dynamic_slice_in_dim(residual, tp_rank * part_width, part_width, 1).astype(
        jnp.float32
    )
    layer_out = (own_resid + mixture).astype(jnp.bfloat16)
    return (layer_out, new_state)


def solution(mesh):
    in_specs = (
        P("ep", None),
        P("ep", "tp", None, None),
        P(None, "tp"),
        P(None, "tp"),
        P(None, "tp"),
        P("tp"),
        P("tp", None),
        P("tp", None),
        P(),
        P(),
        P(),
        P(),
        P("ep", None),
        P("ep", None, "tp"),
        P("ep", None, "tp"),
        P("ep", None, "tp"),
    )
    out_specs = (P("ep", "tp"), P("ep", "tp", None, None))
    return jax.shard_map(local, mesh=mesh, in_specs=in_specs, out_specs=out_specs, check_vma=False)
```

profile of v0, /device:TPU:0, one launch (start us, length us, event | category | flops | bytes accessed | tf_op | source)
XLA Modules:
  0.0 71.4 jit_solution(7429910828382578727)
XLA Ops:
  0.7 0.9 %copy.77 = s32[16,6]{1,0:T(8,128)S(1)} copy(s32[16,6]{0,1:T(8,128)} %param.28) | data formatting | bytes 768 | tf_op args[12]
  2.2 0.7 multiply_add_fusion.1
  3.0 0.9 %fusion.20 = f32[16]{0:T(128)S(1)} fusion(bf16[16,1024]{1,0:T(8,128)(2,1)} %param.16), kind=kLoop, calls=%fused_computation.37 | loop fusion | flops 49136 | bytes 32832 | tf_op jit(solution)/shard_map/reduce_sum | solution.py:10
  3.9 1.3 %divide_multiply_fusion = f32[16,256]{1,0:T(8,128)S(1)} fusion(bf16[1024,256]{1,0:T(8,128)(2,1)} %param.18, bf16[16,1024]{1,0:T(8,128)(2,1)} %param.16, f32[1024]{0:T(1024)} %param.24, f32[16]{0:T(128)S(1)} %add_rsqrt_fusion.2), kind=kOutput, calls=%fused_computation.53 | convolution fusion | flops 8470528 | bytes 577600 | tf_op jit(solution)/shard_map/dot_general | solution.py:38
  5.3 1.3 %fusion.33 = f32[16,256]{1,0:T(8,128)S(1)} fusion(bf16[1024,256]{1,0:T(8,128)(2,1)} %param.20, bf16[16,1024]{1,0:T(8,128)(2,1)} %param.16, f32[1024]{0:T(1024)} %param.24, f32[16]{0:T(128)S(1)} %add_rsqrt_fusion.2), kind=kOutput, calls=%fused_computation.67 | convolution fusion | flops 8454144 | bytes 577600 | tf_op jit(solution)/shard_map/dot_general | solution.py:40
  6.6 0.7 broadcast_subtract_fusion.1
  7.3 1.3 %fusion.8 = f32[16,256]{1,0:T(8,128)S(1)} fusion(bf16[1024,256]{1,0:T(8,128)(2,1)} %param.19, f32[256]{0:T(256)S(1)} %broadcast_subtract_fusion.1, f32[256]{0:T(256)} %param.21, bf16[16,1024]{1,0:T(8,128)(2,1)} %param.16, f32[1024]{0:T(1024)} %param.24, f32[16]{0:T(128)S(1)} %add_rsqrt_fusion.2), kind=kOutput, calls=%fused_computation.16 | convolution fusion | flops 8474624 | bytes 579648 | tf_op jit(solution)/shard_map/dot_general | solution.py:39
  8.7 3.0 %multiply_reduce_fusion = (f32[16,2,128]{2,1,0:T(2,128)S(1)}, f32[16,2,128,128]{3,2,1,0:T(8,128)}) fusion(f32[16,2,128]{2,1,0:T(2,128)S(1)} %mul.173, f32[16,2,128]{2,1,0:T(2,128)S(1)} %mul.169, f32[16,2,128]{2,1,0:T(2,128)S(1)} %broadcast_subtract_fusion, f32[16,2,128,128]{3,2,1,0:T(8,128)S(1)} %copy-done.1, f32[16,2,128]{2,1,0:T(2,128)S(1)} %mul.165), kind=kLoop, calls=%fused_computation.1 | loop fusion | flops 2617344 | bytes 4276224 | tf_op jit(solution)/shard_map/reduce_sum | solution.py:47
  12.0 1.2 %convolution_convert_fusion.2 = bf16[16,1024]{1,0:T(8,128)(2,1)S(1)} fusion(bf16[256,1024]{1,0:T(8,128)(2,1)} %param.23, f32[2,8,2,128]{3,2,1,0:T(2,128)S(1)} %bitcast.43, f32[256]{0:T(256)S(1)} %bitcast.47), kind=kOutput, calls=%fused_computation.10 | convolution fusion | flops 8413184 | bytes 574464 | tf_op jit(solution)/shard_map/dot_general | solution.py:53
  13.2 10.0 %psum.7 = bf16[16,1024]{1,0:T(8,128)(2,1)S(1)} all-reduce(bf16[16,1024]{1,0:T(8,128)(2,1)S(1)} %convolution_convert_fusion.2), channel_id=1, replica_groups=mesh['ep'=16,'tp'=2] {'tp'}, use_global_device_ids=true, to_apply=%region_3.4 | all-reduce | flops 16384 | bytes 65536 | tf_op jit(solution)/shard_map/psum | solution.py:54
  23.6 0.9 %reshape.168 = bf16[16,12,1024]{2,1,0:T(8,128)(2,1)} reshape(bf16[192,1024]{1,0:T(8,128)(2,1)S(1)} %convolution_convert_fusion) | data formatting | bytes 786432 | tf_op jit(solution)/shard_map/reshape | solution.py:89
  24.5 5.9 %all-to-all-start = ((bf16[16,12,1024]{2,1,0:T(8,128)(2,1)}), bf16[16,12,1024]{2,1,0:T(8,128)(2,1)S(1)}, u32[]{:S(2)}, u32[]{:S(2)}) async-start(bf16[16,12,1024]{2,1,0:T(8,128)(2,1)} %reshape.168), calls=%async_computation | async-start | bytes 1048576 | tf_op jit(solution)/shard_map/all_to_all | solution.py:91
  31.1 13.6 %all-to-all-done = bf16[16,12,1024]{2,1,0:T(8,128)(2,1)S(1)} async-done(((bf16[16,12,1024]{2,1,0:T(8,128)(2,1)}), bf16[16,12,1024]{2,1,0:T(8,128)(2,1)S(1)}, u32[]{:S(2)}, u32[]{:S(2)}) %all-to-all-start) | async-done | bytes 393248 | tf_op jit(solution)/shard_map/all_to_all | solution.py:91
  44.8 0.4 fusion.11
  45.2 0.4 fusion.1
  45.6 7.6 %all-gather = bf16[192,1024]{1,0:T(8,128)(2,1)S(1)} all-gather(bf16[192,512]{1,0:T(8,128)(2,1)S(1)} %fusion.1), channel_id=2, replica_groups=mesh['ep'=16,'tp'=2] {'tp'}, dimensions={1}, use_global_device_ids=true | all-gather | bytes 589824 | tf_op jit(solution)/shard_map/all_gather | solution.py:99
  53.2 0.4 fusion.2
  53.6 0.3 copy.92
  53.9 0.5 broadcast.119
  54.4 1.8 %reduce.1 = bf16[192,512]{1,0:T(8,128)(2,1)S(1)} reduce(bf16[192,1,512]{2,1,0:T(2,128)(2,1)S(1)} %bitcast.41, bf16[]{:T(256)} %broadcast.119), dimensions={1}, to_apply=%bitcast.40.reduce_sub_computation | reduce | bytes 393218
  56.3 0.8 %reshape.179 = bf16[16,2,3072]{2,1,0:T(2,128)(2,1)} reshape(bf16[192,512]{1,0:T(8,128)(2,1)S(1)} %reduce.1) | data formatting | bytes 393216
  57.0 4.4 %all-to-all-start.1 = ((bf16[16,2,3072]{2,1,0:T(2,128)(2,1)}), bf16[16,2,3072]{2,1,0:T(2,128)(2,1)S(1)}, u32[]{:S(2)}, u32[]{:S(2)}) async-start(bf16[16,2,3072]{2,1,0:T(2,128)(2,1)} %reshape.179), calls=%async_computation.1 | async-start | bytes 393216 | tf_op jit(solution)/shard_map/all_to_all | solution.py:103
  61.7 8.7 %all-to-all-done.1 = bf16[16,2,3072]{2,1,0:T(2,128)(2,1)S(1)} async-done(((bf16[16,2,3072]{2,1,0:T(2,128)(2,1)}), bf16[16,2,3072]{2,1,0:T(2,128)(2,1)S(1)}, u32[]{:S(2)}, u32[]{:S(2)}) %all-to-all-start.1) | async-done | bytes 196640 | tf_op jit(solution)/shard_map/all_to_all | solution.py:103
  70.8 0.6 add_convert_fusion
  (53 shorter events, 2.9 us)
Async XLA Ops:
  0.6 44.2 %copy-start = (bf16[1,1024,512]{2,1,0:T(8,128)(2,1)S(1)}, bf16[1,1024,512]{2,1,0:T(8,128)(2,1)}, u32[]{:S(2)}) copy-start(bf16[1,1024,512]{2,1,0:T(8,128)(2,1)} %param.29) | copy-start | bytes 3145732
  0.6 8.0 %copy-start.1 = (f32[16,2,128,128]{3,2,1,0:T(8,128)S(1)}, f32[16,2,128,128]{3,2,1,0:T(8,128)}, u32[]{:S(2)}) copy-start(f32[16,2,128,128]{3,2,1,0:T(8,128)} %param.17) | copy-start | bytes 6291460
  8.6 3.4 %copy-start.6 = (f32[2,128]{1,0:T(2,128)S(1)}, f32[2,128]{1,0:T(2,128)}, u32[]{:S(2)}) copy-start(f32[2,128]{1,0:T(2,128)} %param.22) | copy-start | bytes 3076
  8.6 14.5 %copy-start.3 = (bf16[16,1024]{1,0:T(8,128)(2,1)S(1)}, bf16[16,1024]{1,0:T(8,128)(2,1)}, u32[]{:S(2)}) copy-start(bf16[16,1024]{1,0:T(8,128)(2,1)} %param.16) | copy-start | bytes 98308
  8.7 14.7 %copy-start.5 = (f32[1024]{0:T(1024)S(1)}, f32[1024]{0:T(1024)}, u32[]{:S(2)}) copy-start(f32[1024]{0:T(1024)} %param.25) | copy-start | bytes 12292
  11.7 18.8 %copy-start.9 = (bf16[1024,4]{0,1:T(4,128)(2,1)S(1)}, bf16[1024,4]{0,1:T(4,128)(2,1)}, u32[]{:S(2)}) copy-start(bf16[1024,4]{0,1:T(4,128)(2,1)} %param.26) | copy-start | bytes 24580
  11.7 19.1 %copy-start.8 = (bf16[1024,16]{0,1:T(8,128)(2,1)S(1)}, bf16[1024,16]{0,1:T(8,128)(2,1)}, u32[]{:S(2)}) copy-start(bf16[1024,16]{0,1:T(8,128)(2,1)} %param.27) | copy-start | bytes 98308
  24.5 20.7 %copy-start.7 = (bf16[1,1024,512]{2,1,0:T(8,128)(2,1)S(1)}, bf16[1,1024,512]{2,1,0:T(8,128)(2,1)}, u32[]{:S(2)}) copy-start(bf16[1,1024,512]{2,1,0:T(8,128)(2,1)} %param.30) | copy-start | bytes 3145732
  24.5 20.2 %all-to-all-start = ((bf16[16,12,1024]{2,1,0:T(8,128)(2,1)}), bf16[16,12,1024]{2,1,0:T(8,128)(2,1)S(1)}, u32[]{:S(2)}, u32[]{:S(2)}) async-start(bf16[16,12,1024]{2,1,0:T(8,128)(2,1)} %reshape.168), calls=%async_computation | async-start | bytes 1048576 | tf_op jit(solution)/shard_map/all_to_all | solution.py:91
  45.2 8.0 %copy-start.2 = (bf16[1,1024,512]{2,1,0:T(8,128)(2,1)S(1)}, bf16[1,1024,512]{2,1,0:T(8,128)(2,1)}, u32[]{:S(2)}) copy-start(bf16[1,1024,512]{2,1,0:T(8,128)(2,1)} %param.31) | copy-start | bytes 3145732
  45.6 15.8 %copy-start.4 = (s32[16,6]{0,1:T(8,128)S(1)}, s32[16,6]{0,1:T(8,128)}, u32[]{:S(2)}) copy-start(s32[16,6]{0,1:T(8,128)} %param.28) | copy-start | bytes 1156
  57.0 13.4 %all-to-all-start.1 = ((bf16[16,2,3072]{2,1,0:T(2,128)(2,1)}), bf16[16,2,3072]{2,1,0:T(2,128)(2,1)S(1)}, u32[]{:S(2)}, u32[]{:S(2)}) async-start(bf16[16,2,3072]{2,1,0:T(2,128)(2,1)} %reshape.179), calls=%async_computation.1 | async-start | bytes 393216 | tf_op jit(solution)/shard_map/all_to_all | solution.py:103
where the time goes:
time: 71.9 us; the launch traced here: 71.4 us
  waiting for transfers between devices  22.3 us (31%)
  blocking collectives  17.6 us (24%)
  starting transfers between devices  10.3 us (14%)
  other arithmetic  8.77 us (12%)
  matrix products  7.21 us (10%)
  local copies, waits for them, and re-layouts  4.28 us (6%)
  between operations  0.95 us (1%)
    all_to_all x1, waiting for transfers between devices, local(): lax.all_to_all(outgoing, 'ep', split_axis=0, concat_axis=1, tiled=True)  13.6 us
    psum x1, blocking collectives, local(): mixed = lax.psum(head_part.astype(jnp.bfloat16), 'tp')  9.95 us
    all_to_all x1, waiting for transfers between devices, local(): lax.all_to_all(produced, 'ep', split_axis=1, concat_axis=0, tiled=True)  8.72 us
    all_gather x1, blocking collectives, local(): lax.all_gather(hidden, 'tp', axis=2, tiled=True)  7.6 us
    all_to_all x1, starting transfers between devices, local(): lax.all_to_all(outgoing, 'ep', split_axis=0, concat_axis=1, tiled=True)  5.92 us
    all_to_all x1, starting transfers between devices, local(): lax.all_to_all(produced, 'ep', split_axis=1, concat_axis=0, tiled=True)  4.41 us
    reduce_sum x1, other arithmetic, local(): readout = jnp.sum(new_state * query[..., None], axis=2)  3.02 us
    unnamed x24, local copies, waits for them, and re-layouts  2.4 us
  transfers between devices with their start and end apart: 2, of which 2 were waited for; matrix products, arithmetic and copies ran while one was open for 1% of the time, Pallas kernels for 0%

commit v1 on v0

v1 whole, which is shorter than its diff:
```python
import functools

import jax
import jax.numpy as jnp
from jax import lax
from jax.experimental import pallas as pl
from jax.experimental.pallas import tpu as pltpu
from jax.sharding import PartitionSpec as P

epsilon = 1e-06
MESH = pl.DeviceIdType.MESH
BF16 = jnp.bfloat16
F32 = jnp.float32


def scaled_rms(values, gain):
    return values * lax.rsqrt(jnp.mean(values * values, axis=-1, keepdims=True) + epsilon) * gain


def dot(a, b):
    return jnp.dot(a, b, preferred_element_type=F32)


def other(index, step, count):
    total, bit = 0, 1
    while bit < count:
        total = total + ((index // bit + (step // bit) % 2) % 2) * bit
        bit *= 2
    return total


def mix_kernel(
    tokens, gain, lower, head_gain, qw, fw, iw, ow, state, new_state, part,
    wq, wf, wi, wo, st, readout, w_sem, in_sem, out_sem, chunks,
):
    seq, heads, size = st.shape[0], st.shape[1], st.shape[2]
    loads = [
        pltpu.make_async_copy(src, dst, w_sem.at[k])
        for k, (src, dst) in enumerate(((fw, wf), (iw, wi), (qw, wq)))
    ]
    for copy in loads:
        copy.start()
    step = seq // chunks
    ins, outs = [], []
    for k in range(chunks):
        rows = pl.ds(k * step, step)
        ins.append(pltpu.make_async_copy(state.at[rows], st.at[rows], in_sem.at[k]))
        outs.append(pltpu.make_async_copy(st.at[rows], new_state.at[rows], out_sem.at[k]))
        ins[k].start()
    out_load = pltpu.make_async_copy(ow, wo, w_sem.at[3])
    out_load.start()
    normed = scaled_rms(tokens[...].astype(F32), gain[...]).astype(BF16)
    loads[0].wait()
    forget_pre = dot(normed, wf[...])
    low = lower[...]
    forget = low + (1.0 - low) * (1.0 / (1.0 + jnp.exp(-forget_pre)))
    forget_t = forget.T
    loads[1].wait()
    value = dot(normed, wi[...])
    loads[2].wait()
    query_pre = dot(normed, wq[...])
    query = query_pre / (1.0 + jnp.exp(-query_pre))
    query_t = query.T
    for k in range(chunks):
        ins[k].wait()
        for t in range(k * step, (k + 1) * step):
            for h in range(heads):
                cols = slice(h * size, (h + 1) * size)
                f = forget_t[cols, t : t + 1]
                q = query_t[cols, t : t + 1]
                v = value[t : t + 1, cols]
                fresh = f * st[t, h] + (1.0 - f) * v
                st[t, h] = fresh
                readout[h, t : t + 1, :] = jnp.sum(fresh * q, axis=0, keepdims=True)
        outs[k].start()
    out_load.wait()
    total = None
    for h in range(heads):
        head_out = scaled_rms(readout[h], head_gain[h : h + 1, :]).astype(BF16)
        term = dot(head_out, wo[h * size : (h + 1) * size, :])
        total = term if total is None else total + term
    part[...] = total.astype(BF16)
    for k in range(chunks):
        outs[k].wait()


def expert_kernel(
    dims, tokens, part, gain, group_t, expert_t, routes, gw, uw, dw, out,
    wg, wu, wd, parts, resid, x, hid, y, p, q, qr, u, v,
    w_sem, a_s, a_r, z_s, z_r, x_s, x_r, d_s, d_r, h_s, h_r,
    b_s, b_r, c_s, c_r, e_s, e_r,
):
    Z, C, X, TP = dims
    seq, width = tokens.shape
    ep, tp = lax.axis_index("ep"), lax.axis_index("tp")
    core, col, row = ep % C, (ep // C) % X, ep // (C * X)
    cols = out.shape[1]
    experts = expert_t.shape[0]
    groups = group_t.shape[0]

    def ep_of(a, b, c):
        return (a * X + b) * C + c

    z_peers = [other(row, s, Z) for s in range(Z)]
    x_peers = [other(col, d, X) for d in range(X)]
    t_peers = [other(tp, d, TP) for d in range(TP)]
    mate = ep_of(row, col, 1 - core)

    barrier = pltpu.get_barrier_semaphore()
    greet = [{"ep": ep_of(a, col, core)} for a in z_peers[1:]]
    greet += [{"ep": ep_of(row, b, core)} for b in x_peers[1:]]
    greet += [{"tp": t} for t in t_peers[1:]] + [{"ep": mate}]
    for who in greet:
        pl.semaphore_signal(barrier, inc=1, device_id=who, device_id_type=MESH)
    loads = [
        pltpu.make_async_copy(src.at[0], dst, w_sem.at[k])
        for k, (src, dst) in enumerate(((gw, wg), (uw, wu), (dw, wd)))
    ]
    for copy in loads:
        copy.start()
    pl.semaphore_wait(barrier, len(greet))

    started = []

    def send(src, dst, s_sem, r_sem, who):
        copy = pltpu.make_async_remote_copy(
            src_ref=src, dst_ref=dst, send_sem=s_sem, recv_sem=r_sem,
            device_id=who, device_id_type=MESH,
        )
        copy.start()
        started.append(copy)
        return copy

    first = [
        send(part, parts.at[tp], a_s.at[d], a_r.at[d], {"tp": t_peers[d]}) for d in range(1, TP)
    ]
    parts[tp] = part[...]
    for copy in first:
        copy.wait_recv()
    mixed = parts[0].astype(F32)
    for j in range(1, TP):
        mixed = mixed + parts[j].astype(F32)
    mixed = mixed.astype(BF16).astype(F32)
    residual = (tokens[...].astype(F32) + mixed).astype(BF16).astype(F32)
    resid[...] = residual
    ffn_in = scaled_rms(residual, gain[...]).astype(BF16)

    contract = (((1,), (1,)), ((), ()))
    group_raw = jnp.exp(
        lax.dot_general(ffn_in, group_t[...], contract, preferred_element_type=F32)
    )
    group_sum = jnp.sum(group_raw, axis=-1, keepdims=True)
    expert_raw = jnp.exp(
        lax.dot_general(ffn_in, expert_t[...], contract, preferred_element_type=F32)
    )
    lane = lax.broadcasted_iota(jnp.int32, (seq, experts), 1)
    per = experts // groups
    prob = jnp.zeros((seq, experts), F32)
    for g in range(groups):
        member = (lane >= g * per) & (lane < (g + 1) * per)
        total = jnp.sum(jnp.where(member, expert_raw, 0.0), axis=-1, keepdims=True)
        share = group_raw[:, g : g + 1] / group_sum
        prob = jnp.where(member, expert_raw / total * share, prob)
    chosen = lane < 0
    for k in range(routes.shape[1]):
        chosen = chosen | (routes[:, k : k + 1] == lane)
    weight = jnp.where(chosen, prob, 0.0)
    gate = weight / jnp.sum(weight, axis=-1, keepdims=True)
    gate_hi = gate.astype(BF16)
    gate_lo = (gate - gate_hi.astype(F32)).astype(BF16)
    extra = x.shape[-1] - width
    tail = [gate_hi.astype(F32), gate_lo.astype(F32)]
    if extra > 2 * experts:
        tail.append(jnp.zeros((seq, extra - 2 * experts), F32))
    x[row, core, col, :, :width] = ffn_in
    x[row, core, col, :, width:] = jnp.concatenate(tail, axis=1).astype(BF16)

    mine = x.at[row, core, col]
    to_z = [None] + [
        send(mine, mine, z_s.at[s], z_r.at[s], {"ep": ep_of(z_peers[s], col, core)})
        for s in range(1, Z)
    ]

    def send_x(s):
        block = x.at[z_peers[s], core, col]
        return [
            send(block, block, x_s.at[s, d], x_r.at[s, d], {"ep": ep_of(row, x_peers[d], core)})
            for d in range(1, X)
        ]

    def send_d(s):
        column = x.at[z_peers[s], core]
        return send(column, column, d_s.at[s], d_r.at[s], {"ep": mate})

    to_x, to_d = [send_x(0)], []

    def pass_on(s):
        for copy in to_x[s]:
            copy.wait_recv()
        to_d.append(send_d(s))

    rows = C * X * seq
    to_h = []

    def expand(s):
        to_d[s].wait_recv()
        block = x[z_peers[s], :, :, :, :width].reshape(rows, width)
        g = dot(block, wg[...])
        up = dot(block, wu[...])
        hid[z_peers[s], tp] = (g / (1.0 + jnp.exp(-g)) * up).astype(BF16)
        piece = hid.at[z_peers[s], tp]
        to_h.append(
            [
                send(piece, piece, h_s.at[s, d], h_r.at[s, d], {"tp": t_peers[d]})
                for d in range(1, TP)
            ]
        )

    for s in range(1, Z):
        if s == 1:
            pass_on(0)
        to_z[s].wait_recv()
        to_x.append(send_x(s))
    if Z == 1:
        pass_on(0)
    loads[0].wait()
    loads[1].wait()
    for s in range(Z):
        if s + 1 < Z:
            pass_on(s + 1)
        expand(s)
    loads[2].wait()

    to_b, to_c, to_e = {}, {}, {}
    half = wd.shape[0] // TP

    def contract_rows(s):
        for copy in to_h[s]:
            copy.wait_recv()
        total = None
        for j in range(TP):
            term = dot(hid[z_peers[s], j], wd[j * half : (j + 1) * half, :])
            total = term if total is None else total + term
        tags = x[z_peers[s], :, :, :, width:].reshape(rows, extra).astype(F32)
        at = lax.broadcasted_iota(jnp.int32, (rows, extra), 1)
        own = (at == ep) | (at == ep + experts)
        scale = jnp.sum(jnp.where(own, tags, 0.0), axis=-1, keepdims=True)
        y[s] = (total * scale).astype(BF16).reshape(C, X, seq, cols)
        to_b[s] = send(y.at[s, 1 - core], p.at[s], b_s.at[s], b_r.at[s], {"ep": mate})

    def join_cores(s):
        to_b[s].wait_recv()
        q[s] = (y[s, core].astype(F32) + p[s].astype(F32)).astype(BF16)
        to_c[s] = [
            send(
                q.at[s, x_peers[d]], qr.at[s, d], c_s.at[s, d], c_r.at[s, d],
                {"ep": ep_of(row, x_peers[d], core)},
            )
            for d in range(1, X)
        ]

    def join_columns(s):
        total = q[s, col].astype(F32)
        for d in range(1, X):
            to_c[s][d - 1].wait_recv()
            total = total + qr[s, d].astype(F32)
        if s == 0:
            return total
        u[s] = total.astype(BF16)
        to_e[s] = send(
            u.at[s], v.at[s], e_s.at[s], e_r.at[s], {"ep": ep_of(z_peers[s], col, core)}
        )

    order = list(range(Z))[::-1]
    order = list(range(1, Z)) + [0]
    result = None
    for k in range(Z + 2):
        if k < Z:
            contract_rows(order[k])
        if 1 <= k < Z + 1:
            join_cores(order[k - 1])
        if k >= 2:
            result = join_columns(order[k - 2])
    for s in range(1, Z):
        to_e[s].wait_recv()
        result = result + v[s].astype(F32)
    own_resid = resid[:, pl.ds(pl.multiple_of(tp * cols, cols), cols)]
    out[...] = (own_resid + result).astype(BF16)
    for copy in started:
        copy.wait_send()


def local(
    dims,
    tokens,
    old_state,
    query_weight,
    forget_weight,
    input_weight,
    lower_bound,
    head_gain,
    out_weight,
    mix_gain,
    ffn_gain,
    group_weight,
    expert_weight,
    routes,
    gate_weight,
    up_weight,
    down_weight,
):
    Z, C, X, TP = dims
    seq, width = tokens.shape
    heads, size = old_state.shape[1], old_state.shape[2]
    experts = expert_weight.shape[1]
    channels = query_weight.shape[1]
    hidden, cols = gate_weight.shape[2], down_weight.shape[2]
    vmem = pl.BlockSpec(memory_space=pltpu.VMEM)
    anywhere = pl.BlockSpec(memory_space=pl.ANY)
    chunks = 4 if seq % 4 == 0 else 1
    dma = pltpu.SemaphoreType.DMA
    new_state, part = pl.pallas_call(
        functools.partial(mix_kernel, chunks=chunks),
        out_shape=(
            jax.ShapeDtypeStruct(old_state.shape, F32),
            jax.ShapeDtypeStruct((seq, width), BF16),
        ),
        in_specs=[vmem] * 4 + [anywhere] * 5,
        out_specs=(anywhere, vmem),
        scratch_shapes=[
            pltpu.VMEM((width, channels), BF16),
            pltpu.VMEM((width, channels), BF16),
            pltpu.VMEM((width, channels), BF16),
            pltpu.VMEM((channels, width), BF16),
            pltpu.VMEM(old_state.shape, F32),
            pltpu.VMEM((heads, seq, size), F32),
            dma((4,)),
            dma((chunks,)),
            dma((chunks,)),
        ],
        name="mix",
    )(
        tokens, mix_gain[None], lower_bound[None], head_gain,
        query_weight, forget_weight, input_weight, out_weight, old_state,
    )
    extra = -(-2 * experts // 128) * 128
    block = (seq, width + extra)
    layer_out = pl.pallas_call(
        functools.partial(expert_kernel, dims),
        out_shape=jax.ShapeDtypeStruct((seq, cols), BF16),
        in_specs=[vmem] * 6 + [anywhere] * 3,
        out_specs=vmem,
        scratch_shapes=[
            pltpu.VMEM((width, hidden), BF16),
            pltpu.VMEM((width, hidden), BF16),
            pltpu.VMEM((hidden * TP, cols), BF16),
            pltpu.VMEM((TP, seq, width), BF16),
            pltpu.VMEM((seq, width), F32),
            pltpu.VMEM((Z, C, X) + block, BF16),
            pltpu.VMEM((Z, TP, C * X * seq, hidden), BF16),
            pltpu.VMEM((Z, C, X, seq, cols), BF16),
            pltpu.VMEM((Z, X, seq, cols), BF16),
            pltpu.VMEM((Z, X, seq, cols), BF16),
            pltpu.VMEM((Z, X, seq, cols), BF16),
            pltpu.VMEM((Z, seq, cols), BF16),
            pltpu.VMEM((Z, seq, cols), BF16),
            dma((3,)),
            dma((TP,)), dma((TP,)),
            dma((Z,)), dma((Z,)),
            dma((Z, X)), dma((Z, X)),
            dma((Z,)), dma((Z,)),
            dma((Z, TP)), dma((Z, TP)),
            dma((Z,)), dma((Z,)),
            dma((Z, X)), dma((Z, X)),
            dma((Z,)), dma((Z,)),
        ],
        compiler_params=pltpu.CompilerParams(collective_id=0, has_side_effects=True),
        name="experts",
    )(
        tokens, part, ffn_gain[None], group_weight.T, expert_weight.T, routes,
        gate_weight, up_weight, down_weight,
    )
    return (layer_out, new_state)


def solution(mesh):
    in_specs = (
        P("ep", None),
        P("ep", "tp", None, None),
        P(None, "tp"),
        P(None, "tp"),
        P(None, "tp"),
        P("tp"),
        P("tp", None),
        P("tp", None),
        P(),
        P(),
        P(),
        P(),
        P("ep", None),
        P("ep", None, "tp"),
        P("ep", None, "tp"),
        P("ep", None, "tp"),
    )
    out_specs = (P("ep", "tp"), P("ep", "tp", None, None))
    ep, tp = mesh.shape["ep"], mesh.shape["tp"]
    cores = 2
    across = tp
    dims = (ep // (cores * across), cores, across, tp)
    body = functools.partial(local, dims)
    return jax.shard_map(body, mesh=mesh, in_specs=in_specs, out_specs=out_specs, check_vma=False)
```

time: 71.9 us -> 43 us (0.60)
  Pallas kernels: 0 us -> 39.4 us
  waiting for transfers between devices: 22.3 us -> 0 us
  blocking collectives: 17.6 us -> 0 us
  starting transfers between devices: 10.3 us -> 0 us
  other arithmetic: 8.77 us -> 0 us
  matrix products: 7.21 us -> 0 us
  local copies, waits for them, and re-layouts: 4.28 us -> 2.69 us
    pallas_call x0 -> x2, Pallas kernels: none -> 39.4 us  [the longest x1 33.1 us: local(): pl.pallas_call(functools.partial(expert_kernel, dims), out_shape=jax.Shap...]
    all_to_all x2 -> x0, waiting for transfers between devices: 22.3 us -> none  [the longest x1 13.6 us: local(): lax.all_to_all(outgoing, 'ep', split_axis=0, concat_axis=1, tiled=True)]
    all_to_all x2 -> x0, starting transfers between devices: 10.3 us -> none  [the longest x1 5.92 us: local(): lax.all_to_all(outgoing, 'ep', split_axis=0, concat_axis=1, tiled=True)]
    psum x1 -> x0, blocking collectives: 9.95 us -> none  [local(): mixed = lax.psum(head_part.astype(jnp.bfloat16), 'tp')]
    all_gather x1 -> x0, blocking collectives: 7.6 us -> none  [local(): lax.all_gather(hidden, 'tp', axis=2, tiled=True)]
    dot_general x11 -> x0, matrix products: 7.21 us -> none  [the longest x1 1.31 us: local(): jnp.dot(normed, query_weight, preferred_element_type=jnp.float32)]
    reduce_sum x7 -> x0, other arithmetic: 4.57 us -> none  [the longest x1 3.02 us: local(): readout = jnp.sum(new_state * query[..., None], axis=2)]
    unnamed x1 -> x0, other arithmetic: 1.8 us -> none
  transfers between devices with their start and end apart: 2 -> 0, of which waited for: 2 -> 0; matrix products, arithmetic and copies ran while one was open for 1% -> 0% of each run, Pallas kernels for 0% -> 0%
where the time goes in v1:
time: 43 us; the launch traced here: 42.7 us
  Pallas kernels  39.4 us (92%)
  local copies, waits for them, and re-layouts  2.69 us (6%)
  between operations  0.65 us (2%)
    pallas_call x1, Pallas kernels, local(): pl.pallas_call(functools.partial(expert_kernel, dims), out_shape=jax.Shap...  33.1 us
    pallas_call x1, Pallas kernels, local(): pl.pallas_call(functools.partial(mix_kernel, chunks=chunks), out_shape=(j...  6.26 us
    unnamed x2, local copies, waits for them, and re-layouts  2.69 us

profile of v1, /device:TPU:0, one launch (start us, length us, event | category | flops | bytes accessed | tf_op | source)
XLA Modules:
  0.0 42.7 jit_solution(10779119401979769636)
XLA Ops:
  0.6 1.4 %copy.18.routes = s32[16,6]{1,0:T(8,128)} copy(s32[16,6]{0,1:T(8,128)} %param.28) | data formatting | bytes 768 | tf_op args[12]
  2.0 6.3 %mix.1 = (f32[16,2,128,128]{3,2,1,0:T(8,128)}, bf16[16,1024]{1,0:T(8,128)(2,1)}) custom-call(bf16[16,1024]{1,0:T(8,128)(2,1)} %tokens.3, f32[1,1024]{1,0:T(1,128)} %bitcast.7, f32[1,256]{1,0:T(1,128)} %bitcast.9, f32[2,128]{1,0:T(2,128)} %head_gain.1, bf16[1024,256]{1,0:T(8,128)(2,1)} %qw.1, bf16[1024,256]{1,0:T(8,128)(2,1)} %fw.1, bf16[1024,256]{1,0:T(8,128)(2,1)} %iw.1, ...), custom_call_target="tpu_custom_call" | custom-call | tf_op jit(solution)/shard_map/mix/pallas_call | solution.py:322
  8.3 33.1 %experts.1 = bf16[16,512]{1,0:T(8,128)(2,1)} custom-call(bf16[16,1024]{1,0:T(8,128)(2,1)} %tokens.3, bf16[16,1024]{1,0:T(8,128)(2,1)} %get-tuple-element.4.part, f32[1,1024]{1,0:T(1,128)} %bitcast.8, bf16[4,1024]{1,0:T(4,128)(2,1)} %bitcast.6, bf16[16,1024]{1,0:T(8,128)(2,1)} %bitcast.5, s32[16,6]{1,0:T(8,128)} %copy.18.routes, bf16[1,1024,512]{2,1,0:T(8,128)(2,1)} %gw.1, ...), custom_call_target="tpu_custom_call" | custom-call | tf_op jit(solution)/shard_map/experts/pallas_call | solution.py:348
  41.4 1.3 %copy.20 = bf16[16,512]{1,0:T(8,128)(2,1)} copy(bf16[16,512]{1,0:T(8,128)(2,1)} %experts.1) | data formatting | bytes 32768

commit v2 on v1

--- a/solution.py
+++ b/solution.py
@@ -85,10 +85,10 @@
 
 
 def expert_kernel(
-    dims, tokens, part, gain, group_t, expert_t, routes, gw, uw, dw, out,
-    wg, wu, wd, parts, resid, x, hid, y, p, q, qr, u, v,
+    dims, tokens, part, gain, group_t, expert_t, routes_t, gw, uw, dw, out,
+    wg, wu, wd, parts, resid, x, hid, y, p, u, v,
     w_sem, a_s, a_r, z_s, z_r, x_s, x_r, d_s, d_r, h_s, h_r,
-    b_s, b_r, c_s, c_r, e_s, e_r,
+    b_s, b_r, e_s, e_r,
 ):
     Z, C, X, TP = dims
     seq, width = tokens.shape
@@ -104,11 +104,12 @@
     z_peers = [other(row, s, Z) for s in range(Z)]
     x_peers = [other(col, d, X) for d in range(X)]
     t_peers = [other(tp, d, TP) for d in range(TP)]
-    mate = ep_of(row, col, 1 - core)
+    c_peers = [other(core, d, C) for d in range(C)]
+    mate = ep_of(row, col, c_peers[1])
 
     barrier = pltpu.get_barrier_semaphore()
     greet = [{"ep": ep_of(a, col, core)} for a in z_peers[1:]]
-    greet += [{"ep": ep_of(row, b, core)} for b in x_peers[1:]]
+    greet += [{"ep": ep_of(row, b, c)} for b in x_peers[1:] for c in c_peers]
     greet += [{"tp": t} for t in t_peers[1:]] + [{"ep": mate}]
     for who in greet:
         pl.semaphore_signal(barrier, inc=1, device_id=who, device_id_type=MESH)
@@ -161,9 +162,10 @@
         total = jnp.sum(jnp.where(member, expert_raw, 0.0), axis=-1, keepdims=True)
         share = group_raw[:, g : g + 1] / group_sum
         prob = jnp.where(member, expert_raw / total * share, prob)
+    named = routes_t[...].astype(F32).T.astype(jnp.int32)
     chosen = lane < 0
-    for k in range(routes.shape[1]):
-        chosen = chosen | (routes[:, k : k + 1] == lane)
+    for k in range(routes_t.shape[0]):
+        chosen = chosen | (named[:, k : k + 1] == lane)
     weight = jnp.where(chosen, prob, 0.0)
     gate = weight / jnp.sum(weight, axis=-1, keepdims=True)
     gate_hi = gate.astype(BF16)
@@ -176,10 +178,11 @@
     x[row, core, col, :, width:] = jnp.concatenate(tail, axis=1).astype(BF16)
 
     mine = x.at[row, core, col]
-    to_z = [None] + [
-        send(mine, mine, z_s.at[s], z_r.at[s], {"ep": ep_of(z_peers[s], col, core)})
-        for s in range(1, Z)
-    ]
+    far_first = list(range(1, Z))[::-1]
+    to_z = {
+        s: send(mine, mine, z_s.at[s], z_r.at[s], {"ep": ep_of(z_peers[s], col, core)})
+        for s in far_first
+    }
 
     def send_x(s):
         block = x.at[z_peers[s], core, col]
@@ -192,15 +195,15 @@
         column = x.at[z_peers[s], core]
         return send(column, column, d_s.at[s], d_r.at[s], {"ep": mate})
 
-    to_x, to_d = [send_x(0)], []
+    to_x, to_d = {0: send_x(0)}, {}
 
     def pass_on(s):
         for copy in to_x[s]:
             copy.wait_recv()
-        to_d.append(send_d(s))
+        to_d[s] = send_d(s)
 
     rows = C * X * seq
-    to_h = []
+    to_h = {}
 
     def expand(s):
         to_d[s].wait_recv()
@@ -209,29 +212,27 @@
         up = dot(block, wu[...])
         hid[z_peers[s], tp] = (g / (1.0 + jnp.exp(-g)) * up).astype(BF16)
         piece = hid.at[z_peers[s], tp]
-        to_h.append(
-            [
-                send(piece, piece, h_s.at[s, d], h_r.at[s, d], {"tp": t_peers[d]})
-                for d in range(1, TP)
-            ]
-        )
-
-    for s in range(1, Z):
-        if s == 1:
-            pass_on(0)
-        to_z[s].wait_recv()
-        to_x.append(send_x(s))
-    if Z == 1:
-        pass_on(0)
+        to_h[s] = [
+            send(piece, piece, h_s.at[s, d], h_r.at[s, d], {"tp": t_peers[d]})
+            for d in range(1, TP)
+        ]
+
+    order = [0] + far_first
+    pass_on(0)
     loads[0].wait()
     loads[1].wait()
-    for s in range(Z):
-        if s + 1 < Z:
-            pass_on(s + 1)
-        expand(s)
+    for s in far_first:
+        to_z[s].wait_recv()
+        to_x[s] = send_x(s)
+    expand(0)
+    for k in range(1, Z + 1):
+        if k < Z:
+            pass_on(order[k])
+        if k > 1:
+            expand(order[k - 1])
     loads[2].wait()
 
-    to_b, to_c, to_e = {}, {}, {}
+    to_b, to_e = {}, {}
     half = wd.shape[0] // TP
 
     def contract_rows(s):
@@ -243,27 +244,23 @@
             total = term if total is None else total + term
         tags = x[z_peers[s], :, :, :, width:].reshape(rows, extra).astype(F32)
         at = lax.broadcasted_iota(jnp.int32, (rows, extra), 1)
-        own = (at == ep) | (at == ep + experts)
-        scale = jnp.sum(jnp.where(own, tags, 0.0), axis=-1, keepdims=True)
+        here = (at == ep) | (at == ep + experts)
+        scale = jnp.sum(jnp.where(here, tags, 0.0), axis=-1, keepdims=True)
         y[s] = (total * scale).astype(BF16).reshape(C, X, seq, cols)
-        to_b[s] = send(y.at[s, 1 - core], p.at[s], b_s.at[s], b_r.at[s], {"ep": mate})
-
-    def join_cores(s):
-        to_b[s].wait_recv()
-        q[s] = (y[s, core].astype(F32) + p[s].astype(F32)).astype(BF16)
-        to_c[s] = [
+        to_b[s] = [
             send(
-                q.at[s, x_peers[d]], qr.at[s, d], c_s.at[s, d], c_r.at[s, d],
-                {"ep": ep_of(row, x_peers[d], core)},
+                y.at[s, c_peers[n // X], x_peers[n % X]], p.at[s, n], b_s.at[s, n], b_r.at[s, n],
+                {"ep": ep_of(row, x_peers[n % X], c_peers[n // X])},
             )
-            for d in range(1, X)
+            for n in list(range(1, C * X))[::-1]
         ]
 
-    def join_columns(s):
-        total = q[s, col].astype(F32)
-        for d in range(1, X):
-            to_c[s][d - 1].wait_recv()
-            total = total + qr[s, d].astype(F32)
+    def join(s):
+        total = y[s, core, col].astype(F32)
+        for copy in to_b[s]:
+            copy.wait_recv()
+        for n in range(1, C * X):
+            total = total + p[s, n].astype(F32)
         if s == 0:
             return total
         u[s] = total.astype(BF16)
@@ -271,16 +268,14 @@
             u.at[s], v.at[s], e_s.at[s], e_r.at[s], {"ep": ep_of(z_peers[s], col, core)}
         )
 
-    order = list(range(Z))[::-1]
-    order = list(range(1, Z)) + [0]
-    result = None
-    for k in range(Z + 2):
+    own = None
+    for k in range(Z + 1):
         if k < Z:
             contract_rows(order[k])
-        if 1 <= k < Z + 1:
-            join_cores(order[k - 1])
-        if k >= 2:
-            result = join_columns(order[k - 2])
+        if k >= 1:
+            done = join(order[k - 1])
+            own = done if order[k - 1] == 0 else own
+    result = own
     for s in range(1, Z):
         to_e[s].wait_recv()
         result = result + v[s].astype(F32)
@@ -359,9 +354,7 @@
             pltpu.VMEM((Z, C, X) + block, BF16),
             pltpu.VMEM((Z, TP, C * X * seq, hidden), BF16),
             pltpu.VMEM((Z, C, X, seq, cols), BF16),
-            pltpu.VMEM((Z, X, seq, cols), BF16),
-            pltpu.VMEM((Z, X, seq, cols), BF16),
-            pltpu.VMEM((Z, X, seq, cols), BF16),
+            pltpu.VMEM((Z, C * X, seq, cols), BF16),
             pltpu.VMEM((Z, seq, cols), BF16),
             pltpu.VMEM((Z, seq, cols), BF16),
             dma((3,)),
@@ -370,14 +363,13 @@
             dma((Z, X)), dma((Z, X)),
             dma((Z,)), dma((Z,)),
             dma((Z, TP)), dma((Z, TP)),
-            dma((Z,)), dma((Z,)),
-            dma((Z, X)), dma((Z, X)),
+            dma((Z, C * X)), dma((Z, C * X)),
             dma((Z,)), dma((Z,)),
         ],
         compiler_params=pltpu.CompilerParams(collective_id=0, has_side_effects=True),
         name="experts",
     )(
-        tokens, part, ffn_gain[None], group_weight.T, expert_weight.T, routes,
+        tokens, part, ffn_gain[None], group_weight.T, expert_weight.T, routes.T,
         gate_weight, up_weight, down_weight,
     )
     return (layer_out, new_state)

time: 43 us -> 39.3 us (0.914)
  Pallas kernels: 39.4 us -> 37 us
  local copies, waits for them, and re-layouts: 2.69 us -> 1.32 us
    pallas_call x1, Pallas kernels: 33.1 us -> 30.8 us  [local(): pl.pallas_call(functools.partial(expert_kernel, dims), out_shape=jax.Shap...]
    unnamed x2 -> x1, local copies, waits for them, and re-layouts: 2.69 us -> 1.32 us
where the time goes in v2:
time: 39.3 us; the launch traced here: 39 us
  Pallas kernels  37 us (94%)
  local copies, waits for them, and re-layouts  1.32 us (3%)
  between operations  0.65 us (2%)
    pallas_call x1, Pallas kernels, local(): pl.pallas_call(functools.partial(expert_kernel, dims), out_shape=jax.Shap...  30.8 us
    pallas_call x1, Pallas kernels, local(): pl.pallas_call(functools.partial(mix_kernel, chunks=chunks), out_shape=(j...  6.26 us
    unnamed x1, local copies, waits for them, and re-layouts  1.32 us

profile of v2, /device:TPU:0, one launch (start us, length us, event | category | flops | bytes accessed | tf_op | source)
XLA Modules:
  0.0 39.0 jit_solution(1120860645942070728)
XLA Ops:
  0.6 6.3 %mix.1 = (f32[16,2,128,128]{3,2,1,0:T(8,128)}, bf16[16,1024]{1,0:T(8,128)(2,1)}) custom-call(bf16[16,1024]{1,0:T(8,128)(2,1)} %tokens.3, f32[1,1024]{1,0:T(1,128)} %bitcast.8, f32[1,256]{1,0:T(1,128)} %bitcast.11, f32[2,128]{1,0:T(2,128)} %head_gain.1, bf16[1024,256]{1,0:T(8,128)(2,1)} %qw.1, bf16[1024,256]{1,0:T(8,128)(2,1)} %fw.1, bf16[1024,256]{1,0:T(8,128)(2,1)} %iw.1, ...), custom_call_target="tpu_custom_call" | custom-call | tf_op jit(solution)/shard_map/mix/pallas_call | solution.py:317
  6.9 30.8 %experts.1 = bf16[16,512]{1,0:T(8,128)(2,1)} custom-call(bf16[16,1024]{1,0:T(8,128)(2,1)} %tokens.3, bf16[16,1024]{1,0:T(8,128)(2,1)} %get-tuple-element.4.part, f32[1,1024]{1,0:T(1,128)} %bitcast.9, bf16[4,1024]{1,0:T(4,128)(2,1)} %bitcast.7, bf16[16,1024]{1,0:T(8,128)(2,1)} %bitcast.6, s32[6,16]{1,0:T(8,128)} %bitcast.10, bf16[1,1024,512]{2,1,0:T(8,128)(2,1)} %gw.1, ...), custom_call_target="tpu_custom_call" | custom-call | tf_op jit(solution)/shard_map/experts/pallas_call | solution.py:343
  37.7 1.3 %copy.19 = bf16[16,512]{1,0:T(8,128)(2,1)} copy(bf16[16,512]{1,0:T(8,128)(2,1)} %experts.1) | data formatting | bytes 32768
